TPU v7x, 32 devices: a whole 2x2x4 slice. The times are simulated.
32 devices in a mesh: ep: 8 (over z, y), tp: 4 (over x, core).
Axes of the slice: x: 2, y: 2, z: 4, core: 2. Of those that a mesh axis runs over, the one named last changes fastest.
Arguments:
- value_in: bfloat16 [4096, 1024], P('ep', 'tp'), may hold values from -6 to 6
- gate_in: bfloat16 [4096, 1024], P('ep', 'tp'), may hold values from -6 to 6
- outer_gate: bfloat16 [4096, 1024], P('ep', 'tp'), may hold values from -6 to 6
- conv_weight: bfloat16 [3, 1024], P(None, 'tp'), may hold values from -3.5 to 3.5
- out_weight: bfloat16 [1024, 2048], P('tp'), may hold values from -0.1875 to 0.1875
- moe_tokens: bfloat16 [4096, 2048], P(('ep', 'tp')), may hold values from -6 to 6
- norm_gain: bfloat16 [2048], replicated, may hold values from 0.099609375 to 1.8984375
- routes: int32 [4096, 2], P(('ep', 'tp')), may hold values from 0 to 7, all different within a row; in each aligned block of 128 rows (0 to 127, 128 to 255, ...) at most 48 rows name the same one
- route_weight: float32 [4096, 2], P(('ep', 'tp')), may hold values from 0.1 to 1
- expert_gate: bfloat16 [8, 2048, 6144], P('ep', None, 'tp'), may hold values from -0.125 to 0.125
- expert_up: bfloat16 [8, 2048, 6144], P('ep', None, 'tp'), may hold values from -0.125 to 0.125
- expert_down: bfloat16 [8, 6144, 2048], P('ep', 'tp'), may hold values from -0.078125 to 0.078125
Outputs:
- mixer_out: bfloat16 [4096, 2048], P(('ep', 'tp'))
- moe_out: bfloat16 [4096, 2048], P(('ep', 'tp'))
Inputs may be any that keep to these rules, and one draw needn't show every extreme that they name: `routes`: each row names 2 different experts. Among the rows of one device no expert is named by more than 48 rows, a bound that some blocks reach.
All inputs are finite; a program needn't handle non-finite values.
Results may differ from a plain program's by a relative error of at most 0.012.
Values may be sent and summed in bfloat16 or wider, within the bound.
A program may use at most 128 MiB of HBM per device.

v0:
```python
import jax
import jax.numpy as jnp
from jax import lax
from jax.sharding import PartitionSpec as P


def extended(x, sides, width):
    for axis, dim in sides:
        size, length = (lax.axis_size(axis), x.shape[dim])
        up = [(i, (i + 1) % size) for i in range(size - 1)]
        down = [(j, i) for i, j in up]
        last = lax.slice_in_dim(x, length - width, length, axis=dim)
        leading = lax.slice_in_dim(x, 0, width, axis=dim)
        before = lax.ppermute(last, axis, up)
        after = lax.ppermute(leading, axis, down)
        x = jnp.concatenate([before, x, after], axis=dim)
    return x


def rounded(values):
    return lax.optimization_barrier(values.astype(jnp.bfloat16)).astype(jnp.float32)


def mixer_half(value_in, gate_in, outer_gate, conv_weight, out_weight):
    product = (value_in.astype(jnp.float32) * gate_in.astype(jnp.float32)).astype(jnp.bfloat16)
    padded = extended(product, (("ep", 0),), 1).astype(jnp.float32)
    taps = conv_weight.astype(jnp.float32)
    convolved = padded[:-2] * taps[0] + padded[1:-1] * taps[1] + padded[2:] * taps[2]
    mixed_rows = (outer_gate.astype(jnp.float32) * convolved).astype(jnp.bfloat16)
    return lax.psum_scatter(
        rounded(jnp.dot(mixed_rows, out_weight, preferred_element_type=jnp.float32)).astype(
            jnp.bfloat16
        ),
        "tp",
        scatter_dimension=0,
        tiled=True,
    )


def expert_half(moe_tokens, norm_gain, routes, route_weight, expert_gate, expert_up, expert_down):
    row_total, top_count = routes.shape
    features = moe_tokens.shape[1]
    local_units = expert_gate.shape[2]
    experts = lax.axis_size("ep")
    capacity = 3 * top_count * row_total // (2 * experts)
    tokens_f32 = moe_tokens.astype(jnp.float32)
    normed = (
        tokens_f32
        * lax.rsqrt(jnp.mean(tokens_f32 * tokens_f32, axis=-1, keepdims=True) + 1e-06)
        * norm_gain.astype(jnp.float32)
    ).astype(jnp.bfloat16)
    flat_ids = routes.reshape(row_total * top_count)
    matches = (flat_ids[:, None] == jnp.arange(experts, dtype=jnp.int32)[None, :]).astype(jnp.int32)
    position = jnp.sum((jnp.cumsum(matches, axis=0) - 1) * matches, axis=1)
    slot_ids = flat_ids * capacity + position
    placement = slot_ids[:, None] == jnp.arange(experts * capacity, dtype=jnp.int32)[None, :]
    placement = (
        placement.reshape(row_total, top_count, experts * capacity).sum(axis=1).astype(jnp.bfloat16)
    )
    outgoing = jnp.einsum("rs,rd->sd", placement, normed, preferred_element_type=jnp.float32)
    outgoing = outgoing.astype(jnp.bfloat16).reshape(experts, capacity, features)
    arrived = lax.all_to_all(outgoing, "ep", split_axis=0, concat_axis=0, tiled=True)
    slot_block = lax.all_gather(arrived[:, None], "tp", axis=1, tiled=True)
    lead = slot_block.shape[:-1]
    flat_rows = slot_block.reshape(-1, features)
    gate_act = jnp.dot(flat_rows, expert_gate[0], preferred_element_type=jnp.float32)
    up_act = jnp.dot(flat_rows, expert_up[0], preferred_element_type=jnp.float32)
    hidden = (jax.nn.silu(gate_act) * up_act).astype(jnp.bfloat16).reshape(lead + (local_units,))
    group_rows = experts * capacity
    group_count = group_rows * lax.axis_size("tp") // group_rows
    selected = hidden
    selected = jnp.swapaxes(selected, 0, 1).reshape(group_count * group_rows, local_units)
    summed_back = lax.psum_scatter(
        rounded(jnp.dot(selected, expert_down[0], preferred_element_type=jnp.float32)).astype(
            jnp.bfloat16
        ),
        "tp",
        scatter_dimension=0,
        tiled=True,
    )
    returned = lax.all_to_all(
        summed_back.reshape(experts, capacity, features),
        "ep",
        split_axis=0,
        concat_axis=0,
        tiled=True,
    )
    picked = returned.reshape(group_rows, features)[slot_ids].reshape(
        row_total, top_count, features
    )
    return jnp.sum(route_weight[..., None] * picked.astype(jnp.float32), axis=1).astype(
        jnp.bfloat16
    )


def body(
    value_in,
    gate_in,
    outer_gate,
    conv_weight,
    out_weight,
    moe_tokens,
    norm_gain,
    routes,
    route_weight,
    expert_gate,
    expert_up,
    expert_down,
):
    mixer_out = mixer_half(value_in, gate_in, outer_gate, conv_weight, out_weight)
    moe_out = expert_half(
        moe_tokens, norm_gain, routes, route_weight, expert_gate, expert_up, expert_down
    )
    return (mixer_out, moe_out)


def solution(mesh):
    placed = (
        P("ep", "tp"),
        P("ep", "tp"),
        P("ep", "tp"),
        P(None, "tp"),
        P("tp", None),
        P(("ep", "tp"), None),
        P(),
        P(("ep", "tp"), None),
        P(("ep", "tp"), None),
        P("ep", None, "tp"),
        P("ep", None, "tp"),
        P("ep", "tp", None),
    )
    return jax.shard_map(
        body,
        mesh=mesh,
        in_specs=placed,
        out_specs=(P(("ep", "tp"), None), P(("ep", "tp"), None)),
        check_vma=False,
    )
```

profile of v0, /device:TPU:0, one launch (start us, length us, event | category | flops | bytes accessed | tf_op | source)
XLA Modules:
  0.0 263.8 jit_solution(1294568977329746764)
XLA Ops:
  7.2 0.0 copy-start
  7.2 0.0 all-gather.3.cloned.1.call-start
  7.2 0.9 copy.22
  8.1 0.1 eq.43
  8.2 0.1 eq.39
  8.4 0.6 reduce-window.6
  9.0 0.2 slice_reduce_fusion
  9.2 0.1 fusion.20
  9.3 0.1 reduce_sum.41
  9.5 0.1 copy.25
  9.6 0.1 convert_reduce_fusion
  9.7 0.7 convert_element_type.78
  10.4 1.2 fusion.5
  11.6 1.7 convolution_convert_fusion.2
  13.3 44.2 %all_to_all.10 = bf16[8,48,2048]{2,1,0:T(8,128)(2,1)} all-to-all(bf16[8,48,2048]{2,1,0:T(8,128)(2,1)S(1)} %bitcast.33), channel_id=1, replica_groups=mesh['ep'=8,'tp'=4] {'ep'}, dimensions={0} | all-to-all | bytes 3145728 | tf_op jit(solution)/shard_map/all_to_all | solution.py:62
  57.5 0.0 all-gather.3.cloned.1.call-update
  57.6 0.0 reduce-scatter.5.cloned.1.call-start
  57.6 45.5 %all-gather.3.cloned.1.call-done = bf16[8,192,2048]{2,1,0:T(8,128)(2,1)} async-done(((bf16[8,48,2048]{2,1,0:T(8,128)(2,1)}), bf16[8,192,2048]{2,1,0:T(8,128)(2,1)}) %all-gather.3.cloned.1.call-update) | async-done | bytes 6291472 | tf_op jit(solution)/shard_map/all_gather | solution.py:63
  103.1 16.0 %fusion.3 = f32[1536,1536]{1,0:T(8,128)} fusion(bf16[1536,2048]{1,0:T(8,128)(2,1)} %bitcast.44, bf16[1,2048,1536]{2,1,0:T(8,128)(2,1)} %param.21), kind=kOutput, calls=%fused_computation.6 | convolution fusion | flops 9663676416 | bytes 22020096 | tf_op jit(solution)/shard_map/dot_general | solution.py:66
  119.1 0.0 slice-done
  119.1 0.0 slice-done.1
  119.1 0.0 copy-done.6
  119.1 13.8 %fusion = bf16[1536,1536]{1,0:T(8,128)(2,1)S(1)} fusion(bf16[1536,2048]{1,0:T(8,128)(2,1)S(1)} %bitcast.45, f32[1536,1536]{1,0:T(8,128)} %fusion.3, bf16[1,2048,1536]{2,1,0:T(8,128)(2,1)S(1)} %bitcast.43), kind=kOutput, calls=%fused_computation.2 | convolution fusion | flops 9677832192 | bytes 26738688 | tf_op jit(solution)/shard_map/dot_general | solution.py:67
  132.9 0.4 copy.26
  133.3 13.8 %convolution_convert_fusion = bf16[1536,2048]{1,0:T(8,128)(2,1)} fusion(bf16[1536,1536]{1,0:T(8,128)(2,1)S(1)} %bitcast.35, bf16[1,1536,2048]{2,1,0:T(8,128)(2,1)} %param.23), kind=kOutput, calls=%fused_computation.3 | convolution fusion | flops 9666822144 | bytes 17301504 | tf_op jit(solution)/shard_map/dot_general | solution.py:74
  147.1 0.0 reduce-scatter.5.cloned.1.call-update
  147.2 0.0 copy-start.5
  147.2 0.0 reduce-scatter.3.cloned.1.call-start
  147.2 0.9 copy-done.1
  148.1 0.1 copy-done.2
  148.2 0.1 multiply_convert_fusion
  148.2 3.4 %collective-permute-start = (bf16[1,256]{1,0:T(2,128)(2,1)S(1)}, bf16[1,256]{1,0:T(2,128)(2,1)S(1)}, u32[]{:S(2)}, u32[]{:S(2)}) collective-permute-start(bf16[1,256]{1,0:T(2,128)(2,1)S(1)} %get-tuple-element.2), channel_id=1, source_target_pairs={{0,4},{4,8},{8,12},{12,16},{16,20},{20,24},{24,28},{1,5},{5,9},{9,... | collective-permute-start | bytes 1544 | tf_op jit(solution)/shard_map/ppermute | solution.py:14
  151.6 1.3 collective-permute-start.1
  152.9 0.0 collective-permute-done
  153.0 4.1 %collective-permute-done.1 = bf16[1,256]{1,0:T(2,128)(2,1)S(1)} collective-permute-done((bf16[1,256]{1,0:T(2,128)(2,1)S(1)}, bf16[1,256]{1,0:T(2,128)(2,1)S(1)}, u32[]{:S(2)}, u32[]{:S(2)}) %collective-permute-start.1) | collective-permute-done | bytes 544 | tf_op jit(solution)/shard_map/ppermute | solution.py:15
  157.1 0.1 maximum_convert_fusion
  157.1 0.0 copy-done
  157.2 0.0 copy-done.3
  157.2 2.2 convolution_convert_fusion.1
  159.3 0.0 reduce-scatter.3.cloned.1.call-update
  159.3 46.8 %reduce-scatter.5.cloned.1.call-done = bf16[384,2048]{1,0:T(8,128)(2,1)} async-done(((bf16[1536,2048]{1,0:T(8,128)(2,1)}), bf16[384,2048]{1,0:T(8,128)(2,1)}) %reduce-scatter.5.cloned.1.call-update) | async-done | bytes 1572880 | tf_op jit(solution)/shard_map/reduce_scatter | solution.py:73
  206.2 5.5 %all-to-all-start.1 = ((bf16[8,48,2048]{2,1,0:T(8,128)(2,1)}), bf16[8,48,2048]{2,1,0:T(8,128)(2,1)S(1)}, u32[]{:S(2)}, u32[]{:S(2)}) async-start(bf16[8,48,2048]{2,1,0:T(8,128)(2,1)} %bitcast.36), calls=%async_computation.3 | async-start | bytes 3145728 | tf_op jit(solution)/shard_map/all_to_all | solution.py:81
  211.7 0.1 mul.114
  211.8 0.1 copy.21
  212.0 36.6 %all-to-all-done.1 = bf16[8,48,2048]{2,1,0:T(8,128)(2,1)S(1)} async-done(((bf16[8,48,2048]{2,1,0:T(8,128)(2,1)}), bf16[8,48,2048]{2,1,0:T(8,128)(2,1)S(1)}, u32[]{:S(2)}, u32[]{:S(2)}) %all-to-all-start.1) | async-done | bytes 1572896 | tf_op jit(solution)/shard_map/all_to_all | solution.py:81
  248.5 2.3 gather_fusion
  250.9 2.4 reshape.104
  253.3 4.0 %multiply_reduce_fusion = bf16[128,2048]{1,0:T(8,128)(2,1)} fusion(f32[128,2,2048]{2,1,0:T(2,128)S(1)} %reshape.104, f32[128,2]{1,0:T(8,128)S(1)} %copy.21), kind=kLoop, calls=%fused_computation.10 | loop fusion | flops 786432 | bytes 2622464 | tf_op jit(solution)/shard_map/reduce_sum | solution.py:91
  (20 shorter events, 0.1 us)
Async XLA Ops:
  7.2 150.0 %copy-start = (bf16[256,2048]{1,0:T(8,128)(2,1)S(1)}, bf16[256,2048]{1,0:T(8,128)(2,1)}, u32[]{:S(2)}) copy-start(bf16[256,2048]{1,0:T(8,128)(2,1)} %param.16) | copy-start | bytes 3145732
  7.2 95.9 %all-gather.3.cloned.1.call-start = ((), (), s32[]{:S(2)}) async-start(), calls=%async_computation.6 | async-start | bytes 7864320 | tf_op jit(solution)/shard_map/all_gather | solution.py:63
  57.5 61.6 %slice-start = ((s8[6291456]{0:T(1024)(128)(4,1)}), s8[2097152]{0:T(1024)(128)(4,1)S(1)}, s32[]{:S(2)}) async-start(s8[6291456]{0:T(1024)(128)(4,1)} %bitcast.42), calls=%async_computation.7 | async-start | bytes 4194304
  57.6 148.6 %reduce-scatter.5.cloned.1.call-start = ((), (), s32[]{:S(2)}) async-start(), calls=%async_computation.5 | async-start | bytes 7864320 | tf_op jit(solution)/shard_map/reduce_scatter | solution.py:73
  103.1 16.1 %slice-start.1 = ((s8[6291456]{0:T(1024)(128)(4,1)}), s8[4194304]{0:T(1024)(128)(4,1)S(1)}, s32[]{:S(2)}) async-start(s8[6291456]{0:T(1024)(128)(4,1)} %bitcast.42), calls=%async_computation.8 | async-start | bytes 8388608
  103.1 16.1 %copy-start.6 = (bf16[8,192,2048]{2,1,0:T(8,128)(2,1)S(1)}, bf16[8,192,2048]{2,1,0:T(8,128)(2,1)}, u32[]{:S(2)}) copy-start(bf16[8,192,2048]{2,1,0:T(8,128)(2,1)} %all-gather.3.cloned.1.call-done) | copy-start | bytes 18874372
  147.1 0.9 copy-start.1
  147.1 1.0 copy-start.2
  147.1 5.8 %copy-start.4 = (bf16[3,256]{1,0:T(4,128)(2,1)S(1)}, bf16[3,256]{1,0:T(4,128)(2,1)}, u32[]{:S(2)}) copy-start(bf16[3,256]{1,0:T(4,128)(2,1)} %param.15) | copy-start | bytes 4612
  147.1 10.0 %copy-start.3 = (bf16[512,256]{1,0:T(8,128)(2,1)S(1)}, bf16[512,256]{1,0:T(8,128)(2,1)}, u32[]{:S(2)}) copy-start(bf16[512,256]{1,0:T(8,128)(2,1)} %param.14) | copy-start | bytes 786436
  147.2 64.7 %copy-start.5 = (f32[128,2]{0,1:T(2,128)S(1)}, f32[128,2]{0,1:T(2,128)}, u32[]{:S(2)}) copy-start(f32[128,2]{0,1:T(2,128)} %param.20) | copy-start | bytes 3076
  147.2 110.1 %reduce-scatter.3.cloned.1.call-start = ((), (), s32[]{:S(2)}) async-start(), calls=%async_computation.4 | async-start | bytes 2621440 | tf_op jit(solution)/shard_map/reduce_scatter | solution.py:30
  148.2 4.7 %collective-permute-start = (bf16[1,256]{1,0:T(2,128)(2,1)S(1)}, bf16[1,256]{1,0:T(2,128)(2,1)S(1)}, u32[]{:S(2)}, u32[]{:S(2)}) collective-permute-start(bf16[1,256]{1,0:T(2,128)(2,1)S(1)} %get-tuple-element.2), channel_id=1, source_target_pairs={{0,4},{4,8},{8,12},{12,16},{16,20},{20,24},{24,28},{1,5},{5,9},{9,... | collective-permute-start | bytes 1544 | tf_op jit(solution)/shard_map/ppermute | solution.py:14
  151.6 5.5 %collective-permute-start.1 = (bf16[1,256]{1,0:T(2,128)(2,1)S(1)}, bf16[1,256]{1,0:T(2,128)(2,1)S(1)}, u32[]{:S(2)}, u32[]{:S(2)}) collective-permute-start(bf16[1,256]{1,0:T(2,128)(2,1)S(1)} %get-tuple-element.3), channel_id=1, source_target_pairs={{4,0},{8,4},{12,8},{16,12},{20,16},{24,20},{28,24},{5,1},{9,5},{13... | collective-permute-start | bytes 1544 | tf_op jit(solution)/shard_map/ppermute | solution.py:15
  206.2 42.4 %all-to-all-start.1 = ((bf16[8,48,2048]{2,1,0:T(8,128)(2,1)}), bf16[8,48,2048]{2,1,0:T(8,128)(2,1)S(1)}, u32[]{:S(2)}, u32[]{:S(2)}) async-start(bf16[8,48,2048]{2,1,0:T(8,128)(2,1)} %bitcast.36), calls=%async_computation.3 | async-start | bytes 3145728 | tf_op jit(solution)/shard_map/all_to_all | solution.py:81
Sparse Core Ops, SparseCore 0:
  57.7 45.3 all-gather.2
  147.3 58.8 reduce-scatter.4
  209.3 31.1 reduce-scatter.2
where the time goes:
time: 264 us
  waiting for transfers between devices  133 us (50%)
  matrix products  47.5 us (18%)
  blocking collectives  44.2 us (17%)
  between operations  13.9 us (5%)
  starting transfers between devices  10.3 us (4%)
  local copies, waits for them, and re-layouts  7.91 us (3%)
  other arithmetic  6.96 us (3%)
    reduce_scatter x1, waiting for transfers between devices, expert_half(): lax.psum_scatter(rounded(jnp.dot(selected, expert_down[0], preferred_elem...  46.8 us
    all_gather x1, waiting for transfers between devices, expert_half(): slot_block = lax.all_gather(arrived[:, None], 'tp', axis=1, tiled=True)  45.5 us
    all_to_all x1, blocking collectives, expert_half(): lax.all_to_all(outgoing, 'ep', split_axis=0, concat_axis=0, tiled=True)  44.2 us
    all_to_all x1, waiting for transfers between devices, expert_half(): lax.all_to_all(summed_back.reshape(experts, capacity, features), 'ep', sp...  36.6 us
    dot_general x1, matrix products, expert_half(): jnp.dot(flat_rows, expert_gate[0], preferred_element_type=jnp.float32)  16 us
    dot_general x1, matrix products, expert_half(): jnp.dot(selected, expert_down[0], preferred_element_type=jnp.float32)  13.8 us
    dot_general x1, matrix products, expert_half(): jnp.dot(flat_rows, expert_up[0], preferred_element_type=jnp.float32)  13.8 us
    all_to_all x1, starting transfers between devices, expert_half(): lax.all_to_all(summed_back.reshape(experts, capacity, features), 'ep', sp...  5.52 us
  transfers between devices with their start and end apart: 6, of which 4 were waited for; matrix products, arithmetic and copies ran while one was open for 4% of the time, Pallas kernels for 0%

commit v1 on v0

--- a/solution.py
+++ b/solution.py
@@ -60,7 +60,9 @@
     outgoing = jnp.einsum("rs,rd->sd", placement, normed, preferred_element_type=jnp.float32)
     outgoing = outgoing.astype(jnp.bfloat16).reshape(experts, capacity, features)
     arrived = lax.all_to_all(outgoing, "ep", split_axis=0, concat_axis=0, tiled=True)
-    slot_block = lax.all_gather(arrived[:, None], "tp", axis=1, tiled=True)
+    part = arrived[:, None]
+    blocks = lax.all_gather(part, "tp")
+    slot_block = jnp.concatenate(blocks, axis=1)
     lead = slot_block.shape[:-1]
     flat_rows = slot_block.reshape(-1, features)
     gate_act = jnp.dot(flat_rows, expert_gate[0], preferred_element_type=jnp.float32)

time: 264 us -> 266 us (level)
  local copies, waits for them, and re-layouts: 7.91 us -> 11.8 us
    reshape x0 -> x1, local copies, waits for them, and re-layouts: none -> 3.53 us  [expert_half(): slot_block = jnp.concatenate(blocks, axis=1)]
    dot_general x1, matrix products: 16 us -> 12.6 us  [expert_half(): jnp.dot(flat_rows, expert_gate[0], preferred_element_type=jnp.float32)]
where the time goes in v1:
time: 266 us
  waiting for transfers between devices  133 us (50%)
  matrix products  45.3 us (17%)
  blocking collectives  44.2 us (17%)
  between operations  14 us (5%)
  local copies, waits for them, and re-layouts  11.8 us (4%)
  starting transfers between devices  10.3 us (4%)
  other arithmetic  6.96 us (3%)
    reduce_scatter x1, waiting for transfers between devices, expert_half(): lax.psum_scatter(rounded(jnp.dot(selected, expert_down[0], preferred_elem...  46.8 us
    all_gather x1, waiting for transfers between devices, expert_half(): blocks = lax.all_gather(part, 'tp')  45.5 us
    all_to_all x1, blocking collectives, expert_half(): lax.all_to_all(outgoing, 'ep', split_axis=0, concat_axis=0, tiled=True)  44.2 us
    all_to_all x1, waiting for transfers between devices, expert_half(): lax.all_to_all(summed_back.reshape(experts, capacity, features), 'ep', sp...  36.6 us
    dot_general x1, matrix products, expert_half(): jnp.dot(flat_rows, expert_up[0], preferred_element_type=jnp.float32)  14.8 us
    dot_general x1, matrix products, expert_half(): jnp.dot(selected, expert_down[0], preferred_element_type=jnp.float32)  14 us
    dot_general x1, matrix products, expert_half(): jnp.dot(flat_rows, expert_gate[0], preferred_element_type=jnp.float32)  12.6 us
    all_to_all x1, starting transfers between devices, expert_half(): lax.all_to_all(summed_back.reshape(experts, capacity, features), 'ep', sp...  5.52 us
  transfers between devices with their start and end apart: 6, of which 4 were waited for; matrix products, arithmetic and copies ran while one was open for 4% of the time, Pallas kernels for 0%

profile of v1, /device:TPU:0, one launch (start us, length us, event | category | flops | bytes accessed | tf_op | source)
XLA Modules:
  0.0 265.5 jit_solution(10810887587579361720)
XLA Ops:
  7.2 0.0 copy-start
  7.2 0.0 all-gather.3.cloned.1.call-start
  7.2 0.9 copy.34
  8.1 0.1 eq.43
  8.2 0.1 eq.39
  8.4 0.6 reduce-window.6
  9.0 0.2 slice_reduce_fusion
  9.2 0.1 fusion.20
  9.3 0.1 reduce_sum.41
  9.5 0.1 copy.37
  9.6 0.1 convert_reduce_fusion
  9.7 0.7 convert_element_type.78
  10.4 1.2 fusion.5
  11.6 1.7 convolution_convert_fusion.2
  13.3 44.2 %all_to_all.10 = bf16[8,48,2048]{2,1,0:T(8,128)(2,1)} all-to-all(bf16[8,48,2048]{2,1,0:T(8,128)(2,1)S(1)} %bitcast.39), channel_id=1, replica_groups=mesh['ep'=8,'tp'=4] {'ep'}, dimensions={0} | all-to-all | bytes 3145728 | tf_op jit(solution)/shard_map/all_to_all | solution.py:62
  57.5 0.0 all-gather.3.cloned.1.call-update
  57.6 0.0 reduce-scatter.5.cloned.1.call-start
  57.6 45.5 %all-gather.3.cloned.1.call-done = bf16[32,48,2048]{2,1,0:T(8,128)(2,1)} async-done(((bf16[8,48,2048]{2,1,0:T(8,128)(2,1)}), bf16[32,48,2048]{2,1,0:T(8,128)(2,1)}) %all-gather.3.cloned.1.call-update) | async-done | bytes 6291472 | tf_op jit(solution)/shard_map/all_gather | solution.py:64
  103.1 3.5 %copy.38 = bf16[8,4,1,48,2048]{4,3,1,0,2:T(8,128)(2,1)S(1)} copy(bf16[8,4,1,48,2048]{4,3,0,1,2:T(8,128)(2,1)} %bitcast.36) | data formatting | bytes 12582912 | tf_op jit(solution)/shard_map/reshape | solution.py:65
  106.6 0.0 slice-done
  106.6 0.5 slice-done.1
  107.1 12.6 %fusion.3 = f32[1536,1536]{1,0:T(8,128)} fusion(bf16[1536,2048]{1,0:T(8,128)(2,1)S(1)} %bitcast.37, bf16[1,2048,1536]{2,1,0:T(8,128)(2,1)S(1)} %bitcast.49), kind=kOutput, calls=%fused_computation.6 | convolution fusion | flops 9663676416 | bytes 22020096 | tf_op jit(solution)/shard_map/dot_general | solution.py:68
  119.7 14.8 %fusion = bf16[1536,1536]{1,0:T(8,128)(2,1)S(1)} fusion(bf16[1536,2048]{1,0:T(8,128)(2,1)S(1)} %bitcast.38, f32[1536,1536]{1,0:T(8,128)} %fusion.3, bf16[1,2048,1536]{2,1,0:T(8,128)(2,1)} %param.22), kind=kOutput, calls=%fused_computation.2 | convolution fusion | flops 9677832192 | bytes 26738688 | tf_op jit(solution)/shard_map/dot_general | solution.py:69
  134.5 0.3 copy.39
  134.8 14.0 %convolution_convert_fusion = bf16[1536,2048]{1,0:T(8,128)(2,1)} fusion(bf16[1536,1536]{1,0:T(8,128)(2,1)S(1)} %bitcast.41, bf16[1,1536,2048]{2,1,0:T(8,128)(2,1)} %param.23), kind=kOutput, calls=%fused_computation.3 | convolution fusion | flops 9666822144 | bytes 17301504 | tf_op jit(solution)/shard_map/dot_general | solution.py:76
  148.8 0.0 reduce-scatter.5.cloned.1.call-update
  148.8 0.0 copy-start.5
  148.8 0.0 reduce-scatter.3.cloned.1.call-start
  148.9 0.9 copy-done.1
  149.7 0.1 copy-done.2
  149.8 0.1 multiply_convert_fusion
  149.9 3.4 %collective-permute-start = (bf16[1,256]{1,0:T(2,128)(2,1)S(1)}, bf16[1,256]{1,0:T(2,128)(2,1)S(1)}, u32[]{:S(2)}, u32[]{:S(2)}) collective-permute-start(bf16[1,256]{1,0:T(2,128)(2,1)S(1)} %get-tuple-element.2), channel_id=1, source_target_pairs={{0,4},{4,8},{8,12},{12,16},{16,20},{20,24},{24,28},{1,5},{5,9},{9,... | collective-permute-start | bytes 1544 | tf_op jit(solution)/shard_map/ppermute | solution.py:14
  153.3 1.3 collective-permute-start.1
  154.6 0.0 copy-done.4
  154.6 0.0 collective-permute-done
  154.6 4.1 %collective-permute-done.1 = bf16[1,256]{1,0:T(2,128)(2,1)S(1)} collective-permute-done((bf16[1,256]{1,0:T(2,128)(2,1)S(1)}, bf16[1,256]{1,0:T(2,128)(2,1)S(1)}, u32[]{:S(2)}, u32[]{:S(2)}) %collective-permute-start.1) | collective-permute-done | bytes 544 | tf_op jit(solution)/shard_map/ppermute | solution.py:15
  158.8 0.1 maximum_convert_fusion
  158.8 2.2 convolution_convert_fusion.1
  161.0 0.0 reduce-scatter.3.cloned.1.call-update
  161.0 46.8 %reduce-scatter.5.cloned.1.call-done = bf16[384,2048]{1,0:T(8,128)(2,1)} async-done(((bf16[1536,2048]{1,0:T(8,128)(2,1)}), bf16[384,2048]{1,0:T(8,128)(2,1)}) %reduce-scatter.5.cloned.1.call-update) | async-done | bytes 1572880 | tf_op jit(solution)/shard_map/reduce_scatter | solution.py:75
  207.9 5.5 %all-to-all-start.1 = ((bf16[8,48,2048]{2,1,0:T(8,128)(2,1)}), bf16[8,48,2048]{2,1,0:T(8,128)(2,1)S(1)}, u32[]{:S(2)}, u32[]{:S(2)}) async-start(bf16[8,48,2048]{2,1,0:T(8,128)(2,1)} %bitcast.42), calls=%async_computation.3 | async-start | bytes 3145728 | tf_op jit(solution)/shard_map/all_to_all | solution.py:83
  213.4 0.1 mul.114
  213.5 0.0 copy-done.5
  213.5 0.1 copy.33
  213.7 36.6 %all-to-all-done.1 = bf16[8,48,2048]{2,1,0:T(8,128)(2,1)S(1)} async-done(((bf16[8,48,2048]{2,1,0:T(8,128)(2,1)}), bf16[8,48,2048]{2,1,0:T(8,128)(2,1)S(1)}, u32[]{:S(2)}, u32[]{:S(2)}) %all-to-all-start.1) | async-done | bytes 1572896 | tf_op jit(solution)/shard_map/all_to_all | solution.py:83
  250.2 2.3 gather_fusion
  252.6 2.4 reshape.104
  254.9 4.0 %multiply_reduce_fusion = bf16[128,2048]{1,0:T(8,128)(2,1)} fusion(f32[128,2,2048]{2,1,0:T(2,128)S(1)} %reshape.104, f32[128,2]{1,0:T(8,128)S(1)} %copy.33), kind=kLoop, calls=%fused_computation.10 | loop fusion | flops 786432 | bytes 2622464 | tf_op jit(solution)/shard_map/reduce_sum | solution.py:93
  (19 shorter events, 0.1 us)
Async XLA Ops:
  7.2 151.7 %copy-start = (bf16[256,2048]{1,0:T(8,128)(2,1)S(1)}, bf16[256,2048]{1,0:T(8,128)(2,1)}, u32[]{:S(2)}) copy-start(bf16[256,2048]{1,0:T(8,128)(2,1)} %param.16) | copy-start | bytes 3145732
  7.2 95.9 %all-gather.3.cloned.1.call-start = ((), (), s32[]{:S(2)}) async-start(), calls=%async_computation.6 | async-start | bytes 7864320 | tf_op jit(solution)/shard_map/all_gather | solution.py:64
  57.5 49.1 %slice-start = ((s8[6291456]{0:T(1024)(128)(4,1)}), s8[2097152]{0:T(1024)(128)(4,1)S(1)}, s32[]{:S(2)}) async-start(s8[6291456]{0:T(1024)(128)(4,1)} %bitcast.48), calls=%async_computation.7 | async-start | bytes 4194304
  57.6 150.3 %reduce-scatter.5.cloned.1.call-start = ((), (), s32[]{:S(2)}) async-start(), calls=%async_computation.5 | async-start | bytes 7864320 | tf_op jit(solution)/shard_map/reduce_scatter | solution.py:75
  103.1 4.0 %slice-start.1 = ((s8[6291456]{0:T(1024)(128)(4,1)}), s8[4194304]{0:T(1024)(128)(4,1)S(1)}, s32[]{:S(2)}) async-start(s8[6291456]{0:T(1024)(128)(4,1)} %bitcast.48), calls=%async_computation.8 | async-start | bytes 8388608
  148.8 0.9 copy-start.1
  148.8 1.0 copy-start.2
  148.8 5.8 %copy-start.4 = (bf16[3,256]{1,0:T(4,128)(2,1)S(1)}, bf16[3,256]{1,0:T(4,128)(2,1)}, u32[]{:S(2)}) copy-start(bf16[3,256]{1,0:T(4,128)(2,1)} %param.15) | copy-start | bytes 4612
  148.8 10.0 %copy-start.3 = (bf16[512,256]{1,0:T(8,128)(2,1)S(1)}, bf16[512,256]{1,0:T(8,128)(2,1)}, u32[]{:S(2)}) copy-start(bf16[512,256]{1,0:T(8,128)(2,1)} %param.14) | copy-start | bytes 786436
  148.8 64.7 %copy-start.5 = (f32[128,2]{0,1:T(2,128)S(1)}, f32[128,2]{0,1:T(2,128)}, u32[]{:S(2)}) copy-start(f32[128,2]{0,1:T(2,128)} %param.20) | copy-start | bytes 3076
  148.8 110.1 %reduce-scatter.3.cloned.1.call-start = ((), (), s32[]{:S(2)}) async-start(), calls=%async_computation.4 | async-start | bytes 2621440 | tf_op jit(solution)/shard_map/reduce_scatter | solution.py:30
  149.9 4.7 %collective-permute-start = (bf16[1,256]{1,0:T(2,128)(2,1)S(1)}, bf16[1,256]{1,0:T(2,128)(2,1)S(1)}, u32[]{:S(2)}, u32[]{:S(2)}) collective-permute-start(bf16[1,256]{1,0:T(2,128)(2,1)S(1)} %get-tuple-element.2), channel_id=1, source_target_pairs={{0,4},{4,8},{8,12},{12,16},{16,20},{20,24},{24,28},{1,5},{5,9},{9,... | collective-permute-start | bytes 1544 | tf_op jit(solution)/shard_map/ppermute | solution.py:14
  153.3 5.5 %collective-permute-start.1 = (bf16[1,256]{1,0:T(2,128)(2,1)S(1)}, bf16[1,256]{1,0:T(2,128)(2,1)S(1)}, u32[]{:S(2)}, u32[]{:S(2)}) collective-permute-start(bf16[1,256]{1,0:T(2,128)(2,1)S(1)} %get-tuple-element.3), channel_id=1, source_target_pairs={{4,0},{8,4},{12,8},{16,12},{20,16},{24,20},{28,24},{5,1},{9,5},{13... | collective-permute-start | bytes 1544 | tf_op jit(solution)/shard_map/ppermute | solution.py:15
  207.9 42.4 %all-to-all-start.1 = ((bf16[8,48,2048]{2,1,0:T(8,128)(2,1)}), bf16[8,48,2048]{2,1,0:T(8,128)(2,1)S(1)}, u32[]{:S(2)}, u32[]{:S(2)}) async-start(bf16[8,48,2048]{2,1,0:T(8,128)(2,1)} %bitcast.42), calls=%async_computation.3 | async-start | bytes 3145728 | tf_op jit(solution)/shard_map/all_to_all | solution.py:83
Sparse Core Ops, SparseCore 0:
  57.7 45.3 all-gather.2
  149.0 58.8 reduce-scatter.4
  211.0 31.1 reduce-scatter.2
